TPU v7x, 32 devices: a whole 2x2x4 slice. The times are simulated.
32 devices in a mesh: grp: 2 (over y), fs: 4 (over z), tp: 4 (over x, core).
Axes of the slice: x: 2, y: 2, z: 4, core: 2. Of those that a mesh axis runs over, the one named last changes fastest.
Arguments:
- tokens: bfloat16 [1792, 2048], P(('grp', 'fs'), 'tp'), parts along dimension 0, may hold values from -6 to 6
- route_ids: int32 [1792, 2], P(('grp', 'fs')), parts along dimension 0, may hold values from 0 to 3, all different within a row; in each aligned block of 224 rows (0 to 223, 224 to 447, ...) at most 168 rows name the same one
- route_weights: float32 [1792, 2], P(('grp', 'fs')), parts along dimension 0, may hold values from 0.25 to 1
- norm_gain: float32 [2048], P('fs'), may hold values from 0.1 to 1.9
- gate_master: float32 [4, 2048, 512], P(None, 'fs', 'tp'), may hold values from -0.125 to 0.125
- up_master: float32 [4, 2048, 512], P(None, 'fs', 'tp'), may hold values from -0.125 to 0.125
- down_master: float32 [4, 2048, 512], P(None, 'fs', 'tp'), may hold values from -0.25 to 0.25
Outputs:
- gate_serve: bfloat16 [8, 2048, 512], P(('grp', 'fs'), None, 'tp'), parts along dimension 0
- up_serve: bfloat16 [8, 2048, 512], P(('grp', 'fs'), None, 'tp'), parts along dimension 0
- down_serve: bfloat16 [8, 2048, 512], P(('grp', 'fs'), None, 'tp'), parts along dimension 0
- moe_output: bfloat16 [1792, 2048], P(('grp', 'fs'), 'tp'), parts along dimension 0
There are 2 independent parts, one for each index of `grp`. A program takes and returns all parts, laid end to end along the dimension named above; an argument that names none is the same for every part. Nothing has to cross between parts.
Inputs may be any that keep to these rules, and one draw needn't show every extreme that they name: `route_ids`: the 2 experts of a row differ; within the rows of one index of fs (aligned blocks of 224 rows) no expert is named more than 168 times.
All inputs are finite; a program needn't handle non-finite values.
Results may differ from a plain program's by a relative error of at most 0.012.
Values may be sent and summed in bfloat16 or wider, within the bound.
A program may use at most 64 MiB of HBM per device.

v0:
```python
import jax
import jax.numpy as jnp
from jax import lax
from jax.sharding import PartitionSpec as P

norm_epsilon = 1e-06


def slot_numbers(route_ids, experts, capacity):
    flat_ids = route_ids.reshape(-1)
    onehot = (flat_ids[:, None] == jnp.arange(experts, dtype=jnp.int32)[None, :]).astype(jnp.int32)
    before = jnp.cumsum(onehot, axis=0) - onehot
    position = jnp.sum(before * onehot, axis=1)
    return (flat_ids * capacity + position).reshape(route_ids.shape)


def local(tokens, route_ids, route_weights, norm_gain, gate_master, up_master, down_master):
    experts = gate_master.shape[0]
    shards = lax.axis_size("fs")
    columns = lax.axis_size("tp")
    per_device = experts // shards
    tok_rows = route_ids.shape[0]
    top_count = route_ids.shape[1]
    local_width = tokens.shape[1]
    model_width = local_width * columns
    capacity = max(2, 3 * tok_rows * top_count // (2 * experts))
    row_gain = norm_gain[None, :, None]
    gate_half = (gate_master * row_gain).astype(jnp.bfloat16)
    up_half = (up_master * row_gain).astype(jnp.bfloat16)
    down_half = down_master.astype(jnp.bfloat16)
    gate_serve, up_serve, down_serve = (
        lax.all_to_all(gate_half, "fs", split_axis=0, concat_axis=1, tiled=True),
        lax.all_to_all(up_half, "fs", split_axis=0, concat_axis=1, tiled=True),
        lax.all_to_all(down_half, "fs", split_axis=0, concat_axis=1, tiled=True),
    )
    slot_ids = slot_numbers(route_ids, experts, capacity)
    slot_range = jnp.arange(experts * capacity, dtype=jnp.int32)
    selects = [
        (slot_ids[:, rank_slot, None] == slot_range[None, :]).astype(jnp.bfloat16)
        for rank_slot in range(top_count)
    ]
    placing = selects[0]
    for extra in selects[1:]:
        placing = placing + extra
    local_values = tokens.astype(jnp.float32)
    squares = lax.psum(jnp.sum(local_values * local_values, axis=1), "tp")
    inverse = lax.rsqrt(squares / model_width + norm_epsilon)[:, None]
    normed = (local_values * inverse).astype(jnp.bfloat16)
    buffer = jnp.einsum("ts,td->sd", placing, normed, preferred_element_type=jnp.float32).astype(
        jnp.bfloat16
    )
    arrived = lax.all_to_all(
        buffer.reshape(shards, per_device * capacity, local_width),
        "fs",
        split_axis=0,
        concat_axis=0,
        tiled=True,
    )
    arrived = arrived.reshape(shards, per_device, capacity, local_width)
    partial_value = lax.all_gather(arrived, "tp", axis=3, tiled=True)
    gate_sum = jnp.einsum(
        "sxcd,xdf->xscf", partial_value, gate_serve, preferred_element_type=jnp.float32
    )
    up_sum = jnp.einsum(
        "sxcd,xdf->xscf", partial_value, up_serve, preferred_element_type=jnp.float32
    )
    hidden = (jax.nn.silu(gate_sum) * up_sum).astype(jnp.bfloat16)
    products = jnp.einsum("xdf,xscf->dsxc", down_serve, hidden, preferred_element_type=jnp.float32)
    summed = lax.psum_scatter(
        products.reshape(local_width * lax.axis_size("tp"), shards * per_device * capacity).astype(
            jnp.bfloat16
        ),
        "tp",
        scatter_dimension=0,
        tiled=True,
    )
    returned = lax.all_to_all(
        summed.reshape(local_width, shards, per_device * capacity),
        "fs",
        split_axis=1,
        concat_axis=1,
        tiled=True,
    )
    returned = returned.reshape(local_width, experts * capacity)
    combined = jnp.zeros((tok_rows, local_width), jnp.float32)
    for rank_slot in range(top_count):
        picked = jnp.einsum(
            "ts,ds->td", selects[rank_slot], returned, preferred_element_type=jnp.float32
        )
        combined = combined + route_weights[:, rank_slot : rank_slot + 1] * picked
    return (gate_serve, up_serve, down_serve, combined.astype(jnp.bfloat16))


def solution(mesh):
    placed = (
        P(("grp", "fs"), "tp"),
        P(("grp", "fs"), None),
        P(("grp", "fs"), None),
        P("fs"),
        P(None, "fs", "tp"),
        P(None, "fs", "tp"),
        P(None, "fs", "tp"),
    )
    return jax.shard_map(
        local,
        mesh=mesh,
        in_specs=placed,
        out_specs=(
            P(("grp", "fs"), None, "tp"),
            P(("grp", "fs"), None, "tp"),
            P(("grp", "fs"), None, "tp"),
            P(("grp", "fs"), "tp"),
        ),
        check_vma=False,
    )
```

profile of v0, /device:TPU:0, one launch (start us, length us, event | category | flops | bytes accessed | tf_op | source)
XLA Modules:
  0.0 170.7 jit_solution(8881094231520576288)
XLA Ops:
  7.2 0.9 copy.17
  8.4 1.2 reduce-window.6
  10.3 0.7 multiply_add_fusion
  11.0 1.1 fusion.5
  12.1 8.4 %psum.7 = f32[224]{0:T(256)S(1)} all-reduce(f32[224]{0:T(256)S(1)} %fusion.5), channel_id=1, replica_groups=mesh['grp'=2,'fs'=4,'tp'=4] {'tp'}, use_global_device_ids=true, to_apply=%region_4.5 | all-reduce | flops 224 | bytes 1792 | tf_op jit(solution)/shard_map/psum | solution.py:46
  20.5 1.5 convolution_convert_fusion.1
  22.0 21.6 %all_to_all.46 = bf16[4,168,512]{2,1,0:T(8,128)(2,1)} all-to-all(bf16[4,168,512]{2,1,0:T(8,128)(2,1)S(1)} %bitcast.48), channel_id=1, replica_groups=mesh['grp'=2,'fs'=4,'tp'=4] {'fs'}, dimensions={0} | all-to-all | bytes 1376256 | tf_op jit(solution)/shard_map/all_to_all | solution.py:52
  43.6 1.0 multiply_convert_fusion
  44.6 16.2 %all_to_all.47 = bf16[4,512,128]{2,1,0:T(8,128)(2,1)S(1)} all-to-all(bf16[4,512,128]{2,1,0:T(8,128)(2,1)S(1)} %get-tuple-element.9), channel_id=1, replica_groups=mesh['grp'=2,'fs'=4,'tp'=4] {'fs'}, dimensions={0} | all-to-all | bytes 1048576 | tf_op jit(solution)/shard_map/all_to_all | solution.py:32
  60.9 3.5 %all-to-all-start.1 = ((bf16[4,512,128]{2,1,0:T(8,128)(2,1)}), bf16[4,512,128]{2,1,0:T(8,128)(2,1)S(1)}, u32[]{:S(2)}, u32[]{:S(2)}) async-start(bf16[4,512,128]{2,1,0:T(8,128)(2,1)} %get-tuple-element.8), calls=%async_computation.1 | async-start | bytes 1048576 | tf_op jit(solution)/shard_map/all_to_all | solution.py:33
  64.4 0.9 convert_element_type.49
  65.2 12.6 %all-to-all-done.1 = bf16[4,512,128]{2,1,0:T(8,128)(2,1)S(1)} async-done(((bf16[4,512,128]{2,1,0:T(8,128)(2,1)}), bf16[4,512,128]{2,1,0:T(8,128)(2,1)S(1)}, u32[]{:S(2)}, u32[]{:S(2)}) %all-to-all-start.1) | async-done | bytes 524320 | tf_op jit(solution)/shard_map/all_to_all | solution.py:33
  77.9 4.1 %all-to-all-start.2 = ((bf16[4,512,128]{2,1,0:T(8,128)(2,1)}), bf16[4,512,128]{2,1,0:T(8,128)(2,1)}, u32[]{:S(2)}, u32[]{:S(2)}) async-start(bf16[4,512,128]{2,1,0:T(8,128)(2,1)} %convert_element_type.49), calls=%async_computation.2 | async-start | bytes 1048576 | tf_op jit(solution)/shard_map/all_to_all | solution.py:34
  82.1 3.5 %fusion.27 = f32[4,168,128]{2,1,0:T(8,128)} fusion(bf16[4,168,2048]{2,1,0:T(8,128)(2,1)} %all-gather.3.cloned.1.call-done, bf16[2048,128,1]{1,0,2:T(8,128)(2,1)S(1)} %bitcast.41), kind=kOutput, calls=%fused_computation.44 | convolution fusion | flops 352321536 | bytes 3620864 | tf_op jit(solution)/shard_map/sxcd,xdf->xscf/dot_general | solution.py:61
  85.7 10.5 %all-to-all-done.2 = bf16[4,512,128]{2,1,0:T(8,128)(2,1)} async-done(((bf16[4,512,128]{2,1,0:T(8,128)(2,1)}), bf16[4,512,128]{2,1,0:T(8,128)(2,1)}, u32[]{:S(2)}, u32[]{:S(2)}) %all-to-all-start.2) | async-done | bytes 524320 | tf_op jit(solution)/shard_map/all_to_all | solution.py:34
  96.1 5.8 %convolution_convert_fusion = bf16[4,168,2048]{2,1,0:T(8,128)(2,1)} fusion(bf16[2048,128,1]{1,0,2:T(8,128)(2,1)} %bitcast.13, bf16[4,168,2048]{2,1,0:T(8,128)(2,1)S(1)} %copy-done, bf16[2048,128,1]{1,0,2:T(8,128)(2,1)} %bitcast.43, f32[4,168,128]{2,1,0:T(8,128)} %fusion.27), kind=kOutput, calls=%fused_computation | convolution fusion | flops 706535424 | bytes 6897664 | tf_op jit(solution)/shard_map/xdf,xscf->dsxc/dot_general | solution.py:68
  102.0 34.5 %reduce-scatter.2.cloned.1.call-done = bf16[512,672]{0,1:T(8,128)(2,1)} async-done(((bf16[2048,672]{0,1:T(8,128)(2,1)}), bf16[512,672]{0,1:T(8,128)(2,1)}) %reduce-scatter.2.cloned.1.call-update) | async-done | bytes 688144 | tf_op jit(solution)/shard_map/reduce_scatter | solution.py:69
  136.5 4.6 %all-to-all-start.4 = ((bf16[512,4,168]{0,2,1:T(8,128)(2,1)}), bf16[512,4,168]{0,2,1:T(8,128)(2,1)S(1)}, u32[]{:S(2)}, u32[]{:S(2)}) async-start(bf16[512,4,168]{0,2,1:T(8,128)(2,1)} %bitcast.47), calls=%async_computation.5 | async-start | bytes 1376256 | tf_op jit(solution)/shard_map/all_to_all | solution.py:77
  141.1 17.8 %all-to-all-done.4 = bf16[512,4,168]{0,2,1:T(8,128)(2,1)S(1)} async-done(((bf16[512,4,168]{0,2,1:T(8,128)(2,1)}), bf16[512,4,168]{0,2,1:T(8,128)(2,1)S(1)}, u32[]{:S(2)}, u32[]{:S(2)}) %all-to-all-start.4) | async-done | bytes 688160 | tf_op jit(solution)/shard_map/all_to_all | solution.py:77
  158.9 0.4 convolution_multiply_fusion.1
  159.3 1.1 fusion.1
  160.4 0.8 copy.25
  161.2 0.8 copy.26
  162.0 1.9 %copy.27 = bf16[1,2048,128]{2,1,0:T(8,128)(2,1)} copy(bf16[1,2048,128]{2,1,0:T(8,128)(2,1)} %bitcast.2) | data formatting | bytes 1048576
  (35 shorter events, 1.1 us)
Async XLA Ops:
  7.2 36.4 %copy-start.7 = (f32[512]{0:T(512)S(1)}, f32[512]{0:T(512)}, u32[]{:S(2)}) copy-start(f32[512]{0:T(512)} %param.10) | copy-start | bytes 6148
  7.2 36.4 %copy-start.5 = (f32[4,512,128]{2,1,0:T(8,128)S(1)}, f32[4,512,128]{2,1,0:T(8,128)}, u32[]{:S(2)}) copy-start(f32[4,512,128]{2,1,0:T(8,128)} %param.11) | copy-start | bytes 3145732
  7.2 36.4 %copy-start.4 = (f32[4,512,128]{2,1,0:T(8,128)S(1)}, f32[4,512,128]{2,1,0:T(8,128)}, u32[]{:S(2)}) copy-start(f32[4,512,128]{2,1,0:T(8,128)} %param.12) | copy-start | bytes 3145732
  7.2 74.9 %all-gather.3.cloned.1.call-start = ((), (), s32[]{:S(2)}) async-start(), calls=%async_computation.7 | async-start | bytes 3440640 | tf_op jit(solution)/shard_map/all_gather | solution.py:60
  43.6 20.8 %copy-start.3 = (f32[4,512,128]{2,1,0:T(8,128)S(1)}, f32[4,512,128]{2,1,0:T(8,128)}, u32[]{:S(2)}) copy-start(f32[4,512,128]{2,1,0:T(8,128)} %param.13) | copy-start | bytes 3145732
  60.9 17.0 %all-to-all-start.1 = ((bf16[4,512,128]{2,1,0:T(8,128)(2,1)}), bf16[4,512,128]{2,1,0:T(8,128)(2,1)S(1)}, u32[]{:S(2)}, u32[]{:S(2)}) async-start(bf16[4,512,128]{2,1,0:T(8,128)(2,1)} %get-tuple-element.8), calls=%async_computation.1 | async-start | bytes 1048576 | tf_op jit(solution)/shard_map/all_to_all | solution.py:33
  77.9 4.2 %copy-start.1 = (bf16[4,512,128]{2,1,0:T(8,128)(2,1)}, bf16[4,512,128]{2,1,0:T(8,128)(2,1)S(1)}, u32[]{:S(2)}) copy-start(bf16[4,512,128]{2,1,0:T(8,128)(2,1)S(1)} %all-to-all-done.1) | copy-start | bytes 1572868
  77.9 18.3 %all-to-all-start.2 = ((bf16[4,512,128]{2,1,0:T(8,128)(2,1)}), bf16[4,512,128]{2,1,0:T(8,128)(2,1)}, u32[]{:S(2)}, u32[]{:S(2)}) async-start(bf16[4,512,128]{2,1,0:T(8,128)(2,1)} %convert_element_type.49), calls=%async_computation.2 | async-start | bytes 1048576 | tf_op jit(solution)/shard_map/all_to_all | solution.py:34
  82.0 54.5 %reduce-scatter.2.cloned.1.call-start = ((), (), s32[]{:S(2)}) async-start(), calls=%async_computation.6 | async-start | bytes 3440640 | tf_op jit(solution)/shard_map/reduce_scatter | solution.py:69
  82.1 14.0 %copy-start = (bf16[4,168,2048]{2,1,0:T(8,128)(2,1)S(1)}, bf16[4,168,2048]{2,1,0:T(8,128)(2,1)}, u32[]{:S(2)}) copy-start(bf16[4,168,2048]{2,1,0:T(8,128)(2,1)} %all-gather.3.cloned.1.call-done) | copy-start | bytes 8257540
  102.0 39.1 %copy-start.6 = (f32[224,2]{0,1:T(2,128)S(1)}, f32[224,2]{0,1:T(2,128)}, u32[]{:S(2)}) copy-start(f32[224,2]{0,1:T(2,128)} %param.9) | copy-start | bytes 5380
  102.0 59.2 %copy-start.2 = (bf16[4,512,128]{2,1,0:T(8,128)(2,1)S(1)}, bf16[4,512,128]{2,1,0:T(8,128)(2,1)}, u32[]{:S(2)}) copy-start(bf16[4,512,128]{2,1,0:T(8,128)(2,1)} %copy-done.1) | copy-start | bytes 1572868
  136.5 22.4 %all-to-all-start.4 = ((bf16[512,4,168]{0,2,1:T(8,128)(2,1)}), bf16[512,4,168]{0,2,1:T(8,128)(2,1)S(1)}, u32[]{:S(2)}, u32[]{:S(2)}) async-start(bf16[512,4,168]{0,2,1:T(8,128)(2,1)} %bitcast.47), calls=%async_computation.5 | async-start | bytes 1376256 | tf_op jit(solution)/shard_map/all_to_all | solution.py:77
Sparse Core Ops, SparseCore 0:
  43.7 25.4 all-gather.2
  102.1 34.3 reduce-scatter.1
where the time goes:
time: 171 us
  waiting for transfers between devices  75.5 us (44%)
  blocking collectives  46.2 us (27%)
  between operations  14.2 us (8%)
  starting transfers between devices  12.3 us (7%)
  matrix products  12.3 us (7%)
  other arithmetic  5.18 us (3%)
  local copies, waits for them, and re-layouts  5.04 us (3%)
    reduce_scatter x1, waiting for transfers between devices, local(): lax.psum_scatter(products.reshape(local_width * lax.axis_size('tp'), shar...  34.5 us
    all_to_all x1, blocking collectives, local(): lax.all_to_all(buffer.reshape(shards, per_device * capacity, local_width)...  21.6 us
    all_to_all x1, waiting for transfers between devices, local(): lax.all_to_all(summed.reshape(local_width, shards, per_device * capacity)...  17.8 us
    all_to_all x1, blocking collectives, local(): lax.all_to_all(gate_half, 'fs', split_axis=0, concat_axis=1, tiled=True)  16.2 us
    all_to_all x1, waiting for transfers between devices, local(): lax.all_to_all(up_half, 'fs', split_axis=0, concat_axis=1, tiled=True)  12.6 us
    all_to_all x1, waiting for transfers between devices, local(): lax.all_to_all(down_half, 'fs', split_axis=0, concat_axis=1, tiled=True)  10.5 us
    psum x1, blocking collectives, local(): squares = lax.psum(jnp.sum(local_values * local_values, axis=1), 'tp')  8.37 us
    dot_general x1, matrix products, local(): jnp.einsum('xdf,xscf->dsxc', down_serve, hidden, preferred_element_type=j...  5.82 us
  transfers between devices with their start and end apart: 5, of which 4 were waited for; matrix products, arithmetic and copies ran while one was open for 3% of the time, Pallas kernels for 0%

commit v1 on v0

--- a/solution.py
+++ b/solution.py
@@ -49,13 +49,20 @@
     buffer = jnp.einsum("ts,td->sd", placing, normed, preferred_element_type=jnp.float32).astype(
         jnp.bfloat16
     )
-    arrived = lax.all_to_all(
-        buffer.reshape(shards, per_device * capacity, local_width),
-        "fs",
-        split_axis=0,
-        concat_axis=0,
-        tiled=True,
-    )
+    array = buffer.reshape(shards, per_device * capacity, local_width)
+    ways, here = (lax.axis_size("fs"), lax.axis_index("fs"))
+    width = array.shape[0] // ways
+    shape = list(array.shape)
+    shape[0] = width
+    height = shape[0]
+    shape[0] = height * ways
+    full = jnp.zeros(shape, array.dtype)
+    for mask in range(ways):
+        part = lax.dynamic_slice_in_dim(array, (here ^ mask) * width, width, axis=0)
+        if mask:
+            part = lax.ppermute(part, "fs", [(d, d ^ mask) for d in range(ways)])
+        full = lax.dynamic_update_slice_in_dim(full, part, (here ^ mask) * height, axis=0)
+    arrived = full
     arrived = arrived.reshape(shards, per_device, capacity, local_width)
     partial_value = lax.all_gather(arrived, "tp", axis=3, tiled=True)
     gate_sum = jnp.einsum(

time: 171 us -> 171 us (level)
  blocking collectives: 46.2 us -> 24.9 us
  waiting for transfers between devices: 75.5 us -> 87.2 us
  starting transfers between devices: 12.3 us -> 16.7 us
  local copies, waits for them, and re-layouts: 5.04 us -> 9.43 us
    all_to_all x2 -> x1, blocking collectives: 37.8 us -> 16.6 us  [local(): lax.all_to_all(up_half, 'fs', split_axis=0, concat_axis=1, tiled=True)]
    ppermute x0 -> x3, waiting for transfers between devices: none -> 11.2 us  [local(): part = lax.ppermute(part, 'fs', [(d, d ^ mask) for d in range(ways)])]
    ppermute x0 -> x3, starting transfers between devices: none -> 4.39 us  [local(): part = lax.ppermute(part, 'fs', [(d, d ^ mask) for d in range(ways)])]
    dynamic_update_slice x0 -> x4, local copies, waits for them, and re-layouts: none -> 2.82 us  [local(): lax.dynamic_update_slice_in_dim(full, part, (here ^ mask) * height, axis=0)]
    unnamed x21 -> x23, local copies, waits for them, and re-layouts: 4.44 us -> 5.15 us
  transfers between devices with their start and end apart: 5 -> 8, of which waited for: 4 -> 6; matrix products, arithmetic and copies ran while one was open for 3% -> 4% of each run, Pallas kernels for 0% -> 0%
where the time goes in v1:
time: 171 us; the launch traced here: 170 us
  waiting for transfers between devices  87.2 us (51%)
  blocking collectives  24.9 us (15%)
  starting transfers between devices  16.7 us (10%)
  between operations  14.3 us (8%)
  matrix products  12.3 us (7%)
  local copies, waits for them, and re-layouts  9.43 us (6%)
  other arithmetic  5.33 us (3%)
    reduce_scatter x1, waiting for transfers between devices, local(): lax.psum_scatter(products.reshape(local_width * lax.axis_size('tp'), shar...  35.2 us
    all_to_all x1, waiting for transfers between devices, local(): lax.all_to_all(summed.reshape(local_width, shards, per_device * capacity)...  17.8 us
    all_to_all x1, blocking collectives, local(): lax.all_to_all(up_half, 'fs', split_axis=0, concat_axis=1, tiled=True)  16.6 us
    all_to_all x1, waiting for transfers between devices, local(): lax.all_to_all(gate_half, 'fs', split_axis=0, concat_axis=1, tiled=True)  12.5 us
    ppermute x3, waiting for transfers between devices, local(): part = lax.ppermute(part, 'fs', [(d, d ^ mask) for d in range(ways)])  11.2 us
    all_to_all x1, waiting for transfers between devices, local(): lax.all_to_all(down_half, 'fs', split_axis=0, concat_axis=1, tiled=True)  10.4 us
    psum x1, blocking collectives, local(): squares = lax.psum(jnp.sum(local_values * local_values, axis=1), 'tp')  8.37 us
    dot_general x1, matrix products, local(): jnp.einsum('xdf,xscf->dsxc', down_serve, hidden, preferred_element_type=j...  5.81 us
  transfers between devices with their start and end apart: 8, of which 6 were waited for; matrix products, arithmetic and copies ran while one was open for 4% of the time, Pallas kernels for 0%

profile of v1, /device:TPU:0, one launch (start us, length us, event | category | flops | bytes accessed | tf_op | source)
XLA Modules:
  0.0 170.1 jit_solution(16203623944920428865)
XLA Ops:
  8.2 1.2 reduce-window.6
  10.9 1.2 fusion.8
  12.1 8.4 %psum.7 = f32[224]{0:T(256)S(1)} all-reduce(f32[224]{0:T(256)S(1)} %fusion.8), channel_id=1, replica_groups=mesh['grp'=2,'fs'=4,'tp'=4] {'tp'}, use_global_device_ids=true, to_apply=%region_4.5 | all-reduce | flops 224 | bytes 1792 | tf_op jit(solution)/shard_map/psum | solution.py:46
  20.5 1.5 convolution_convert_fusion.1
  22.8 1.6 collective-permute-start
  24.4 2.6 %collective-permute-start.1 = (bf16[1,168,512]{2,1,0:T(8,128)(2,1)}, bf16[1,168,512]{2,1,0:T(8,128)(2,1)}, u32[]{:S(2)}, u32[]{:S(2)}) collective-permute-start(bf16[1,168,512]{2,1,0:T(8,128)(2,1)} %get-tuple-element.5), channel_id=1, source_target_pairs={{0,8},{4,12},{8,0},{12,4},{1,9},{5,13},{9,1},{13,5},{2,10},{6,14},... | collective-permute-start | bytes 516104 | tf_op jit(solution)/shard_map/ppermute | solution.py:63
  27.2 3.3 %collective-permute-done = bf16[1,168,512]{2,1,0:T(8,128)(2,1)} collective-permute-done((bf16[1,168,512]{2,1,0:T(8,128)(2,1)}, bf16[1,168,512]{2,1,0:T(8,128)(2,1)}, u32[]{:S(2)}, u32[]{:S(2)}) %collective-permute-start) | collective-permute-done | bytes 172064 | tf_op jit(solution)/shard_map/ppermute | solution.py:63
  30.6 0.9 bitcast_dynamic-update-slice_fusion.1
  31.5 7.9 %collective-permute-done.1 = bf16[1,168,512]{2,1,0:T(8,128)(2,1)} collective-permute-done((bf16[1,168,512]{2,1,0:T(8,128)(2,1)}, bf16[1,168,512]{2,1,0:T(8,128)(2,1)}, u32[]{:S(2)}, u32[]{:S(2)}) %collective-permute-start.1) | collective-permute-done | bytes 172064 | tf_op jit(solution)/shard_map/ppermute | solution.py:63
  39.4 0.9 bitcast_dynamic-update-slice_fusion
  40.4 0.9 bitcast_dynamic-update-slice_fusion.2
  42.2 1.0 multiply_convert_fusion
  43.3 16.6 %all_to_all.41 = bf16[4,512,128]{2,1,0:T(8,128)(2,1)S(1)} all-to-all(bf16[4,512,128]{2,1,0:T(8,128)(2,1)S(1)} %get-tuple-element.11), channel_id=1, replica_groups=mesh['grp'=2,'fs'=4,'tp'=4] {'fs'}, dimensions={0} | all-to-all | bytes 1048576 | tf_op jit(solution)/shard_map/all_to_all | solution.py:33
  59.8 3.5 %all-to-all-start = ((bf16[4,512,128]{2,1,0:T(8,128)(2,1)}), bf16[4,512,128]{2,1,0:T(8,128)(2,1)S(1)}, u32[]{:S(2)}, u32[]{:S(2)}) async-start(bf16[4,512,128]{2,1,0:T(8,128)(2,1)} %get-tuple-element.12), calls=%async_computation | async-start | bytes 1048576 | tf_op jit(solution)/shard_map/all_to_all | solution.py:32
  64.2 12.5 %all-to-all-done = bf16[4,512,128]{2,1,0:T(8,128)(2,1)S(1)} async-done(((bf16[4,512,128]{2,1,0:T(8,128)(2,1)}), bf16[4,512,128]{2,1,0:T(8,128)(2,1)S(1)}, u32[]{:S(2)}, u32[]{:S(2)}) %all-to-all-start) | async-done | bytes 524320 | tf_op jit(solution)/shard_map/all_to_all | solution.py:32
  76.7 4.1 %all-to-all-start.2 = ((bf16[4,512,128]{2,1,0:T(8,128)(2,1)}), bf16[4,512,128]{2,1,0:T(8,128)(2,1)}, u32[]{:S(2)}, u32[]{:S(2)}) async-start(bf16[4,512,128]{2,1,0:T(8,128)(2,1)} %convert_element_type.49), calls=%async_computation.2 | async-start | bytes 1048576 | tf_op jit(solution)/shard_map/all_to_all | solution.py:34
  81.0 3.5 %fusion = f32[4,168,128]{2,1,0:T(8,128)} fusion(bf16[2048,128,1]{1,0,2:T(8,128)(2,1)S(1)} %bitcast.60, bf16[4,1,168,2048]{3,2,0,1:T(8,128)(2,1)} %all-gather.2.cloned.1.call-done), kind=kOutput, calls=%fused_computation.1 | convolution fusion | flops 352321536 | bytes 3620864 | tf_op jit(solution)/shard_map/sxcd,xdf->xscf/dot_general | solution.py:71
  84.5 10.4 %all-to-all-done.2 = bf16[4,512,128]{2,1,0:T(8,128)(2,1)} async-done(((bf16[4,512,128]{2,1,0:T(8,128)(2,1)}), bf16[4,512,128]{2,1,0:T(8,128)(2,1)}, u32[]{:S(2)}, u32[]{:S(2)}) %all-to-all-start.2) | async-done | bytes 524320 | tf_op jit(solution)/shard_map/all_to_all | solution.py:34
  94.9 5.8 %convolution_convert_fusion = bf16[4,168,2048]{2,1,0:T(8,128)(2,1)} fusion(bf16[2048,128,1]{1,0,2:T(8,128)(2,1)} %bitcast.20, f32[4,168,128]{2,1,0:T(8,128)} %fusion, bf16[2048,128,1]{1,0,2:T(8,128)(2,1)} %bitcast.62, bf16[4,1,168,2048]{3,2,0,1:T(8,128)(2,1)S(1)} %copy-done), kind=kOutput, calls=%fused_computation | convolution fusion | flops 706535424 | bytes 6897664 | tf_op jit(solution)/shard_map/xdf,xscf->dsxc/dot_general | solution.py:75
  100.8 35.2 %reduce-scatter.2.cloned.1.call-done = bf16[512,672]{0,1:T(8,128)(2,1)} async-done(((bf16[2048,672]{0,1:T(8,128)(2,1)}), bf16[512,672]{0,1:T(8,128)(2,1)}) %reduce-scatter.2.cloned.1.call-update) | async-done | bytes 688144 | tf_op jit(solution)/shard_map/reduce_scatter | solution.py:76
  135.9 4.6 %all-to-all-start.3 = ((bf16[512,4,168]{0,2,1:T(8,128)(2,1)}), bf16[512,4,168]{0,2,1:T(8,128)(2,1)S(1)}, u32[]{:S(2)}, u32[]{:S(2)}) async-start(bf16[512,4,168]{0,2,1:T(8,128)(2,1)} %bitcast.66), calls=%async_computation.4 | async-start | bytes 1376256 | tf_op jit(solution)/shard_map/all_to_all | solution.py:84
  140.5 17.8 %all-to-all-done.3 = bf16[512,4,168]{0,2,1:T(8,128)(2,1)S(1)} async-done(((bf16[512,4,168]{0,2,1:T(8,128)(2,1)}), bf16[512,4,168]{0,2,1:T(8,128)(2,1)S(1)}, u32[]{:S(2)}, u32[]{:S(2)}) %all-to-all-start.3) | async-done | bytes 688160 | tf_op jit(solution)/shard_map/all_to_all | solution.py:84
  158.8 1.1 fusion.5
  161.4 1.9 %copy.39 = bf16[1,2048,128]{2,1,0:T(8,128)(2,1)} copy(bf16[1,2048,128]{2,1,0:T(8,128)(2,1)} %bitcast.2) | data formatting | bytes 1048576
  (48 shorter events, 7.4 us)
Async XLA Ops:
  7.2 73.8 %all-gather.2.cloned.1.call-start = ((), (), s32[]{:S(2)}) async-start(), calls=%async_computation.5 | async-start | bytes 3440640 | tf_op jit(solution)/shard_map/all_gather | solution.py:67
  10.9 31.3 %copy-start.5 = (f32[4,512,128]{2,1,0:T(8,128)S(1)}, f32[4,512,128]{2,1,0:T(8,128)}, u32[]{:S(2)}) copy-start(f32[4,512,128]{2,1,0:T(8,128)} %param.12) | copy-start | bytes 3145732
  10.9 31.3 %copy-start.6 = (f32[4,512,128]{2,1,0:T(8,128)S(1)}, f32[4,512,128]{2,1,0:T(8,128)}, u32[]{:S(2)}) copy-start(f32[4,512,128]{2,1,0:T(8,128)} %param.11) | copy-start | bytes 3145732
  10.9 31.3 %copy-start.8 = (f32[512]{0:T(512)S(1)}, f32[512]{0:T(512)}, u32[]{:S(2)}) copy-start(f32[512]{0:T(512)} %param.10) | copy-start | bytes 6148
  22.8 7.8 %collective-permute-start = (bf16[1,168,512]{2,1,0:T(8,128)(2,1)}, bf16[1,168,512]{2,1,0:T(8,128)(2,1)}, u32[]{:S(2)}, u32[]{:S(2)}) collective-permute-start(bf16[1,168,512]{2,1,0:T(8,128)(2,1)} %get-tuple-element.6), channel_id=1, source_target_pairs={{0,4},{4,0},{8,12},{12,8},{1,5},{5,1},{9,13},{13,9},{2,6},{6,2},{1... | collective-permute-start | bytes 516104 | tf_op jit(solution)/shard_map/ppermute | solution.py:63
  24.4 15.1 %collective-permute-start.1 = (bf16[1,168,512]{2,1,0:T(8,128)(2,1)}, bf16[1,168,512]{2,1,0:T(8,128)(2,1)}, u32[]{:S(2)}, u32[]{:S(2)}) collective-permute-start(bf16[1,168,512]{2,1,0:T(8,128)(2,1)} %get-tuple-element.5), channel_id=1, source_target_pairs={{0,8},{4,12},{8,0},{12,4},{1,9},{5,13},{9,1},{13,5},{2,10},{6,14},... | collective-permute-start | bytes 516104 | tf_op jit(solution)/shard_map/ppermute | solution.py:63
  27.0 13.4 %collective-permute-start.2 = (bf16[1,168,512]{2,1,0:T(8,128)(2,1)}, bf16[1,168,512]{2,1,0:T(8,128)(2,1)}, u32[]{:S(2)}, u32[]{:S(2)}) collective-permute-start(bf16[1,168,512]{2,1,0:T(8,128)(2,1)} %get-tuple-element.4), channel_id=1, source_target_pairs={{0,12},{4,8},{8,4},{12,0},{1,13},{5,9},{9,5},{13,1},{2,14},{6,10},... | collective-permute-start | bytes 516104 | tf_op jit(solution)/shard_map/ppermute | solution.py:63
  41.3 0.9 copy-start.3
  42.2 21.1 %copy-start.4 = (f32[4,512,128]{2,1,0:T(8,128)S(1)}, f32[4,512,128]{2,1,0:T(8,128)}, u32[]{:S(2)}) copy-start(f32[4,512,128]{2,1,0:T(8,128)} %param.13) | copy-start | bytes 3145732
  59.8 16.9 %all-to-all-start = ((bf16[4,512,128]{2,1,0:T(8,128)(2,1)}), bf16[4,512,128]{2,1,0:T(8,128)(2,1)S(1)}, u32[]{:S(2)}, u32[]{:S(2)}) async-start(bf16[4,512,128]{2,1,0:T(8,128)(2,1)} %get-tuple-element.12), calls=%async_computation | async-start | bytes 1048576 | tf_op jit(solution)/shard_map/all_to_all | solution.py:32
  76.7 4.2 %copy-start.1 = (bf16[4,512,128]{2,1,0:T(8,128)(2,1)}, bf16[4,512,128]{2,1,0:T(8,128)(2,1)S(1)}, u32[]{:S(2)}) copy-start(bf16[4,512,128]{2,1,0:T(8,128)(2,1)S(1)} %all-to-all-done) | copy-start | bytes 1572868
  76.7 18.2 %all-to-all-start.2 = ((bf16[4,512,128]{2,1,0:T(8,128)(2,1)}), bf16[4,512,128]{2,1,0:T(8,128)(2,1)}, u32[]{:S(2)}, u32[]{:S(2)}) async-start(bf16[4,512,128]{2,1,0:T(8,128)(2,1)} %convert_element_type.49), calls=%async_computation.2 | async-start | bytes 1048576 | tf_op jit(solution)/shard_map/all_to_all | solution.py:34
  80.9 55.0 %reduce-scatter.2.cloned.1.call-start = ((), (), s32[]{:S(2)}) async-start(), calls=%async_computation.6 | async-start | bytes 3440640 | tf_op jit(solution)/shard_map/reduce_scatter | solution.py:76
  81.0 14.0 %copy-start = (bf16[4,1,168,2048]{3,2,0,1:T(8,128)(2,1)S(1)}, bf16[4,1,168,2048]{3,2,0,1:T(8,128)(2,1)}, u32[]{:S(2)}) copy-start(bf16[4,1,168,2048]{3,2,0,1:T(8,128)(2,1)} %all-gather.2.cloned.1.call-done) | copy-start | bytes 8257540
  100.7 39.8 %copy-start.7 = (f32[224,2]{0,1:T(2,128)S(1)}, f32[224,2]{0,1:T(2,128)}, u32[]{:S(2)}) copy-start(f32[224,2]{0,1:T(2,128)} %param.9) | copy-start | bytes 5380
  100.7 59.1 %copy-start.2 = (bf16[4,512,128]{2,1,0:T(8,128)(2,1)S(1)}, bf16[4,512,128]{2,1,0:T(8,128)(2,1)}, u32[]{:S(2)}) copy-start(bf16[4,512,128]{2,1,0:T(8,128)(2,1)} %copy-done.1) | copy-start | bytes 1572868
  135.9 22.4 %all-to-all-start.3 = ((bf16[512,4,168]{0,2,1:T(8,128)(2,1)}), bf16[512,4,168]{0,2,1:T(8,128)(2,1)S(1)}, u32[]{:S(2)}, u32[]{:S(2)}) async-start(bf16[512,4,168]{0,2,1:T(8,128)(2,1)} %bitcast.66), calls=%async_computation.4 | async-start | bytes 1376256 | tf_op jit(solution)/shard_map/all_to_all | solution.py:84
Sparse Core Ops, SparseCore 0:
  42.3 26.4 all-gather.1
  100.9 34.9 reduce-scatter.1
